TPU v7x, 512 devices: a whole 4x8x8 slice. The times are simulated.
512 devices in a mesh: gr: 2 (over z_hi), fs: 32 (over z_lo, y), tp: 8 (over x, core).
Axes of the slice: x: 4, y: 8, z: 8 (z_hi: 2, z_lo: 4; z = z_hi * 4 + z_lo), core: 2. Of those that a mesh axis runs over, the one named last changes fastest.
Arguments:
- prompt: bfloat16 [16, 256, 2048], P(('gr', 'tp')), as said below
- norm_gain: float32 [2, 2048], P(None, 'fs'), may hold values from 0.1 to 1.9
- gate_weight: float32 [2, 2048, 4096], P(None, 'fs', ('gr', 'tp')), may hold values from -0.125 to 0.125
- up_weight: float32 [2, 2048, 4096], P(None, 'fs', ('gr', 'tp')), may hold values from -0.125 to 0.125
- down_weight: float32 [2, 4096, 2048], P(None, 'fs', ('gr', 'tp')), may hold values from -0.09375 to 0.09375
Outputs:
- gate_sampler: bfloat16 [2, 2048, 4096], P(None, None, 'fs')
- up_sampler: bfloat16 [2, 2048, 4096], P(None, None, 'fs')
- down_sampler: bfloat16 [2, 4096, 2048], P(None, 'fs')
- mixed: bfloat16 [16, 256, 2048], P(('gr', 'tp'))
Inputs may be any that keep to these rules, and one draw needn't show every extreme that they name: prompt features have scales that differ from feature to feature.
All inputs are finite; a program needn't handle non-finite values.
Results may differ from a plain program's by a relative error of at most 0.0043.
Values may be sent and summed in bfloat16 or wider, within the bound.
No kernel may reach another device: no remote copies, remote signals or barrier semaphores. Data moves between devices by JAX's collectives and lax.ppermute only.
A program may use at most 64 MiB of HBM per device.

v0:
```python
import jax
import jax.numpy as jnp
from jax import lax
from jax.sharding import PartitionSpec as P

norm_eps = 1e-06


def side_by_side(arrays, axis, dim, along):
    both = jnp.concatenate(arrays, axis=along)
    whole, at, finished = (lax.all_gather(both, axis, axis=dim, tiled=True), 0, [])
    for a in arrays:
        finished.append(lax.slice_in_dim(whole, at, at + a.shape[along], axis=along))
        at += a.shape[along]
    return tuple(finished)


def in_blocks(value, dim, count):
    shape = value.shape
    tiles = value.reshape(*shape[:dim], count, shape[dim] // count, *shape[dim + 1 :])
    return jnp.moveaxis(tiles, dim, 0)


def sum_at_owner(value, axis, dim):
    count = lax.axis_size(axis)
    tiles = lax.all_to_all(in_blocks(value, dim, count), axis, 0, 0, tiled=True)
    return jnp.sum(tiles.astype(jnp.float32), axis=0)


def from_everyone(value, axis):
    count = lax.axis_size(axis)
    return lax.all_to_all(
        jnp.broadcast_to(value[None], (count, *value.shape)), axis, 0, 0, tiled=True
    )


def taken_together(value, axis):
    everything = from_everyone(value, axis)
    return jnp.sum(everything, axis=0)


def laid_out(tiles, dim):
    shape = list(tiles.shape[1:])
    shape[dim] *= tiles.shape[0]
    return jnp.moveaxis(tiles, 0, dim).reshape(shape)


def gather_directly(value, axis, dim):
    return laid_out(from_everyone(value, axis), dim)


def per_device(prompt, norm_gain, gate_weight, up_weight, down_weight):
    width = prompt.shape[2]
    stream = prompt.reshape(-1, width).astype(jnp.float32)
    normed = (
        stream * lax.rsqrt(jnp.mean(stream * stream, axis=-1, keepdims=True) + norm_eps)
    ).astype(jnp.bfloat16)
    col_count = width // lax.axis_size("fs")
    col_start = lax.axis_index("fs") * col_count
    columns = lax.dynamic_slice_in_dim(stream, col_start, col_count, 1)
    mixed = prompt
    gate_list = []
    up_list = []
    down_list = []
    for half_step in range(2):
        gain_col = norm_gain[half_step][:, None]
        gate_bf = (gain_col * gate_weight[half_step]).astype(jnp.bfloat16)
        up_bf = (gain_col * up_weight[half_step]).astype(jnp.bfloat16)
        down_bf = down_weight[half_step].astype(jnp.bfloat16)
        gate_all, up_all, down_new = (
            *side_by_side((gate_bf, up_bf), ("gr", "tp"), 1, 0),
            lax.all_gather(down_bf, ("gr", "tp"), axis=1, tiled=True),
        )
        gate_new, up_new = (
            lax.all_to_all(gate_all, "fs", split_axis=1, concat_axis=0, tiled=True),
            lax.all_to_all(up_all, "fs", split_axis=1, concat_axis=0, tiled=True),
        )
        gate_list.append(gate_new)
        up_list.append(up_new)
        down_list.append(down_new)
        gate_act = jnp.dot(normed, gate_new, preferred_element_type=jnp.float32)
        up_act = jnp.dot(normed, up_new, preferred_element_type=jnp.float32)
        hidden = (jax.nn.silu(gate_act) * up_act).astype(jnp.bfloat16)
        partial_value = jnp.dot(hidden, down_new, preferred_element_type=jnp.float32)
        summed = sum_at_owner(partial_value.astype(jnp.bfloat16), "fs", 1)
        columns = columns + 0.5 * summed
        if half_step == 0:
            squares = taken_together(jnp.sum(columns * columns, axis=1, keepdims=True), "fs")
            normed_part = (columns * lax.rsqrt(squares / width + norm_eps)).astype(jnp.bfloat16)
            normed = gather_directly(normed_part, "fs", 1)
        else:
            mixed = gather_directly(columns.astype(jnp.bfloat16), "fs", 1).reshape(prompt.shape)
    return (jnp.stack(gate_list), jnp.stack(up_list), jnp.stack(down_list), mixed)


def solution(mesh):
    in_specs = (
        P(("gr", "tp"), None, None),
        P(None, "fs"),
        P(None, "fs", ("gr", "tp")),
        P(None, "fs", ("gr", "tp")),
        P(None, "fs", ("gr", "tp")),
    )
    out_specs = (
        P(None, None, "fs"),
        P(None, None, "fs"),
        P(None, "fs", None),
        P(("gr", "tp"), None, None),
    )
    return jax.shard_map(
        per_device, mesh=mesh, in_specs=in_specs, out_specs=out_specs, check_vma=False
    )
```

profile of v0, /device:TPU:8, one launch (start us, length us, event | category | flops | bytes accessed | tf_op | source)
XLA Modules:
  0.0 410.3 jit_solution(2993411757497262500)
XLA Ops:
  7.2 0.8 slice_bitcast_fusion.5
  8.0 1.0 fusion.28
  9.0 0.6 pad_maximum_fusion.3
  9.7 68.5 %all-gather.5.cloned.1.call-done = bf16[128,4096]{1,0:T(8,128)(2,1)} async-done(((bf16[128,256]{1,0:T(8,128)(2,1)}), bf16[128,4096]{1,0:T(8,128)(2,1)}) %all-gather.5.cloned.1.call-update) | async-done | bytes 1048592 | tf_op jit(solution)/shard_map/all_gather | solution.py:11
  78.1 1.3 slice_bitcast_fusion.1
  79.4 0.9 copy.47
  80.3 7.9 %all-to-all-start = ((bf16[64,32,128]{2,0,1:T(8,128)(2,1)}), bf16[64,32,128]{2,0,1:T(8,128)(2,1)S(1)}, u32[]{:S(2)}, u32[]{:S(2)}) async-start(bf16[64,32,128]{2,0,1:T(8,128)(2,1)} %bitcast.101), calls=%async_computation | async-start | bytes 1048576 | tf_op jit(solution)/shard_map/all_to_all | solution.py:75
  88.2 1.5 copy.32
  89.7 0.9 copy.45
  90.7 15.5 %all-to-all-done = bf16[64,32,128]{2,0,1:T(8,128)(2,1)S(1)} async-done(((bf16[64,32,128]{2,0,1:T(8,128)(2,1)}), bf16[64,32,128]{2,0,1:T(8,128)(2,1)S(1)}, u32[]{:S(2)}, u32[]{:S(2)}) %all-to-all-start) | async-done | bytes 524320 | tf_op jit(solution)/shard_map/all_to_all | solution.py:75
  106.1 4.7 %all-to-all-start.2 = ((bf16[64,32,128]{2,0,1:T(8,128)(2,1)}), bf16[64,32,128]{2,0,1:T(8,128)(2,1)S(1)}, u32[]{:S(2)}, u32[]{:S(2)}) async-start(bf16[64,32,128]{2,0,1:T(8,128)(2,1)} %bitcast.99), calls=%async_computation.2 | async-start | bytes 1048576 | tf_op jit(solution)/shard_map/all_to_all | solution.py:76
  110.9 0.3 multiply_reduce_fusion
  111.2 30.8 %all-gather = bf16[1,128,2048]{2,1,0:T(8,128)(2,1)S(1)} all-gather(bf16[1,128,128]{2,1,0:T(8,128)(2,1)S(1)} %get-tuple-element.26), channel_id=2, replica_groups=mesh['gr'=2,'fs'=32,'tp'=8] {'gr','tp'}, dimensions={2}, use_global_device_ids=true | all-gather | bytes 557056 | tf_op jit(solution)/shard_map/all_gather | solution.py:72
  142.0 0.5 fusion.9
  142.5 0.8 convolution_convert_fusion.1
  143.4 1.3 copy.33
  144.7 13.4 %all-to-all-start.4 = ((bf16[32,256,64]{1,2,0:T(8,128)(2,1)}), bf16[32,256,64]{1,2,0:T(8,128)(2,1)S(1)}, u32[]{:S(2)}, u32[]{:S(2)}) async-start(bf16[32,256,64]{1,2,0:T(8,128)(2,1)} %bitcast.105), calls=%async_computation.4 | async-start | bytes 2097152 | tf_op jit(solution)/shard_map/all_to_all | solution.py:26
  158.1 0.6 pad_maximum_fusion.4
  158.7 0.1 all-gather.7.cloned.1.call-update
  158.8 1.5 convert_element_type.63
  160.3 26.9 %all-to-all-done.4 = bf16[32,256,64]{1,2,0:T(8,128)(2,1)S(1)} async-done(((bf16[32,256,64]{1,2,0:T(8,128)(2,1)}), bf16[32,256,64]{1,2,0:T(8,128)(2,1)S(1)}, u32[]{:S(2)}, u32[]{:S(2)}) %all-to-all-start.4) | async-done | bytes 1048608 | tf_op jit(solution)/shard_map/all_to_all | solution.py:26
  187.2 0.2 convert_reduce_fusion.1
  187.4 0.9 multiply_reduce_fusion.1
  188.2 0.6 broadcast_in_dim.6
  188.9 6.1 %all-to-all-start.5 = ((f32[32,256,1]{1,2,0:T(1,128)}), f32[32,256,1]{1,2,0:T(1,128)S(1)}, u32[]{:S(2)}, u32[]{:S(2)}) async-start(f32[32,256,1]{1,2,0:T(1,128)} %broadcast_in_dim.6), calls=%async_computation.5 | async-start | bytes 65536 | tf_op jit(solution)/shard_map/all_to_all | solution.py:32
  195.0 26.7 %all-gather.7.cloned.1.call-done = bf16[128,4096]{1,0:T(8,128)(2,1)} async-done(((bf16[128,256]{1,0:T(8,128)(2,1)}), bf16[128,4096]{1,0:T(8,128)(2,1)}) %all-gather.7.cloned.1.call-update) | async-done | bytes 1048592 | tf_op jit(solution)/shard_map/all_gather | solution.py:11
  221.7 1.3 slice_bitcast_fusion
  223.0 0.9 copy.46
  223.9 7.9 %all-to-all-start.1 = ((bf16[64,32,128]{2,0,1:T(8,128)(2,1)}), bf16[64,32,128]{2,0,1:T(8,128)(2,1)S(1)}, u32[]{:S(2)}, u32[]{:S(2)}) async-start(bf16[64,32,128]{2,0,1:T(8,128)(2,1)} %bitcast.100), calls=%async_computation.1 | async-start | bytes 1048576 | tf_op jit(solution)/shard_map/all_to_all | solution.py:75
  231.9 17.8 %all-to-all-done.1 = bf16[64,32,128]{2,0,1:T(8,128)(2,1)S(1)} async-done(((bf16[64,32,128]{2,0,1:T(8,128)(2,1)}), bf16[64,32,128]{2,0,1:T(8,128)(2,1)S(1)}, u32[]{:S(2)}, u32[]{:S(2)}) %all-to-all-start.1) | async-done | bytes 524320 | tf_op jit(solution)/shard_map/all_to_all | solution.py:75
  249.7 1.1 broadcast_in_dim.7
  250.8 4.7 %all-to-all-start.6 = ((bf16[32,256,64]{1,2,0:T(8,128)(2,1)}), bf16[32,256,64]{1,2,0:T(8,128)(2,1)S(1)}, u32[]{:S(2)}, u32[]{:S(2)}) async-start(bf16[32,256,64]{1,2,0:T(8,128)(2,1)} %broadcast_in_dim.7), calls=%async_computation.6 | async-start | bytes 2097152 | tf_op jit(solution)/shard_map/all_to_all | solution.py:32
  255.6 0.9 copy.44
  256.5 27.6 %all-to-all-done.6 = bf16[32,256,64]{1,2,0:T(8,128)(2,1)S(1)} async-done(((bf16[32,256,64]{1,2,0:T(8,128)(2,1)}), bf16[32,256,64]{1,2,0:T(8,128)(2,1)S(1)}, u32[]{:S(2)}, u32[]{:S(2)}) %all-to-all-start.6) | async-done | bytes 1048608 | tf_op jit(solution)/shard_map/all_to_all | solution.py:32
  284.1 5.0 %all-to-all-start.3 = ((bf16[64,32,128]{2,0,1:T(8,128)(2,1)}), bf16[64,32,128]{2,0,1:T(8,128)(2,1)S(1)}, u32[]{:S(2)}, u32[]{:S(2)}) async-start(bf16[64,32,128]{2,0,1:T(8,128)(2,1)} %bitcast.98), calls=%async_computation.3 | async-start | bytes 1048576 | tf_op jit(solution)/shard_map/all_to_all | solution.py:76
  289.2 31.4 %all-gather.1 = bf16[1,128,2048]{2,1,0:T(8,128)(2,1)S(1)} all-gather(bf16[1,128,128]{2,1,0:T(8,128)(2,1)S(1)} %get-tuple-element.27), channel_id=3, replica_groups=mesh['gr'=2,'fs'=32,'tp'=8] {'gr','tp'}, dimensions={2}, use_global_device_ids=true | all-gather | bytes 557056 | tf_op jit(solution)/shard_map/all_gather | solution.py:72
  320.5 1.5 convolution_bitcast_fusion.1
  322.1 1.8 convolution_convert_fusion
  323.9 1.5 copy.34
  325.4 42.0 %all_to_all.95 = bf16[32,256,64]{1,2,0:T(8,128)(2,1)S(1)} all-to-all(bf16[32,256,64]{1,2,0:T(8,128)(2,1)S(1)} %bitcast.107), channel_id=1, replica_groups=mesh['gr'=2,'fs'=32,'tp'=8] {'fs'}, dimensions={0} | all-to-all | bytes 2097152 | tf_op jit(solution)/shard_map/all_to_all | solution.py:26
  367.4 0.2 convert_reduce_fusion
  367.5 1.1 broadcast_in_dim.8
  368.6 5.0 %all-to-all-start.8 = ((bf16[32,256,64]{1,2,0:T(8,128)(2,1)}), bf16[32,256,64]{1,2,0:T(8,128)(2,1)S(1)}, u32[]{:S(2)}, u32[]{:S(2)}) async-start(bf16[32,256,64]{1,2,0:T(8,128)(2,1)} %broadcast_in_dim.8), calls=%async_computation.8 | async-start | bytes 2097152 | tf_op jit(solution)/shard_map/all_to_all | solution.py:32
  373.6 1.1 pad_maximum_fusion.2
  374.7 1.1 pad_maximum_fusion.1
  375.7 1.1 pad_maximum_fusion
  376.8 25.3 %all-to-all-done.8 = bf16[32,256,64]{1,2,0:T(8,128)(2,1)S(1)} async-done(((bf16[32,256,64]{1,2,0:T(8,128)(2,1)}), bf16[32,256,64]{1,2,0:T(8,128)(2,1)S(1)}, u32[]{:S(2)}, u32[]{:S(2)}) %all-to-all-start.8) | async-done | bytes 1048608 | tf_op jit(solution)/shard_map/all_to_all | solution.py:32
  402.1 1.4 copy.35
  (23 shorter events, 0.2 us)
Async XLA Ops:
  7.2 70.9 %all-gather.5.cloned.1.call-start = ((), (), s32[]{:S(2)}) async-start(), calls=%async_computation.9 | async-start | bytes 1114112 | tf_op jit(solution)/shard_map/all_gather | solution.py:11
  80.3 25.8 %all-to-all-start = ((bf16[64,32,128]{2,0,1:T(8,128)(2,1)}), bf16[64,32,128]{2,0,1:T(8,128)(2,1)S(1)}, u32[]{:S(2)}, u32[]{:S(2)}) async-start(bf16[64,32,128]{2,0,1:T(8,128)(2,1)} %bitcast.101), calls=%async_computation | async-start | bytes 1048576 | tf_op jit(solution)/shard_map/all_to_all | solution.py:75
  89.7 21.5 %copy-start.4 = (f32[2,128,128]{2,1,0:T(8,128)S(1)}, f32[2,128,128]{2,1,0:T(8,128)}, u32[]{:S(2)}) copy-start(f32[2,128,128]{2,1,0:T(8,128)} %param.9) | copy-start | bytes 393220
  106.1 36.4 %copy-start = (bf16[64,32,128]{2,0,1:T(8,128)(2,1)}, bf16[64,32,128]{2,0,1:T(8,128)(2,1)S(1)}, u32[]{:S(2)}) copy-start(bf16[64,32,128]{2,0,1:T(8,128)(2,1)S(1)} %all-to-all-done) | copy-start | bytes 1572868
  106.1 36.4 %all-to-all-start.2 = ((bf16[64,32,128]{2,0,1:T(8,128)(2,1)}), bf16[64,32,128]{2,0,1:T(8,128)(2,1)S(1)}, u32[]{:S(2)}, u32[]{:S(2)}) async-start(bf16[64,32,128]{2,0,1:T(8,128)(2,1)} %bitcast.99), calls=%async_computation.2 | async-start | bytes 1048576 | tf_op jit(solution)/shard_map/all_to_all | solution.py:76
  144.7 42.5 %all-to-all-start.4 = ((bf16[32,256,64]{1,2,0:T(8,128)(2,1)}), bf16[32,256,64]{1,2,0:T(8,128)(2,1)S(1)}, u32[]{:S(2)}, u32[]{:S(2)}) async-start(bf16[32,256,64]{1,2,0:T(8,128)(2,1)} %bitcast.105), calls=%async_computation.4 | async-start | bytes 2097152 | tf_op jit(solution)/shard_map/all_to_all | solution.py:26
  158.1 63.6 %all-gather.7.cloned.1.call-start = ((), (), s32[]{:S(2)}) async-start(), calls=%async_computation.10 | async-start | bytes 1114112 | tf_op jit(solution)/shard_map/all_gather | solution.py:11
  188.9 35.0 %all-to-all-start.5 = ((f32[32,256,1]{1,2,0:T(1,128)}), f32[32,256,1]{1,2,0:T(1,128)S(1)}, u32[]{:S(2)}, u32[]{:S(2)}) async-start(f32[32,256,1]{1,2,0:T(1,128)} %broadcast_in_dim.6), calls=%async_computation.5 | async-start | bytes 65536 | tf_op jit(solution)/shard_map/all_to_all | solution.py:32
  223.9 25.8 %all-to-all-start.1 = ((bf16[64,32,128]{2,0,1:T(8,128)(2,1)}), bf16[64,32,128]{2,0,1:T(8,128)(2,1)S(1)}, u32[]{:S(2)}, u32[]{:S(2)}) async-start(bf16[64,32,128]{2,0,1:T(8,128)(2,1)} %bitcast.100), calls=%async_computation.1 | async-start | bytes 1048576 | tf_op jit(solution)/shard_map/all_to_all | solution.py:75
  249.7 6.8 %copy-start.2 = (bf16[64,32,128]{2,0,1:T(8,128)(2,1)}, bf16[64,32,128]{2,0,1:T(8,128)(2,1)S(1)}, u32[]{:S(2)}) copy-start(bf16[64,32,128]{2,0,1:T(8,128)(2,1)S(1)} %all-to-all-done.1) | copy-start | bytes 1572868
  250.8 33.3 %all-to-all-start.6 = ((bf16[32,256,64]{1,2,0:T(8,128)(2,1)}), bf16[32,256,64]{1,2,0:T(8,128)(2,1)S(1)}, u32[]{:S(2)}, u32[]{:S(2)}) async-start(bf16[32,256,64]{1,2,0:T(8,128)(2,1)} %broadcast_in_dim.7), calls=%async_computation.6 | async-start | bytes 2097152 | tf_op jit(solution)/shard_map/all_to_all | solution.py:32
  284.1 38.0 %all-to-all-start.3 = ((bf16[64,32,128]{2,0,1:T(8,128)(2,1)}), bf16[64,32,128]{2,0,1:T(8,128)(2,1)S(1)}, u32[]{:S(2)}, u32[]{:S(2)}) async-start(bf16[64,32,128]{2,0,1:T(8,128)(2,1)} %bitcast.98), calls=%async_computation.3 | async-start | bytes 1048576 | tf_op jit(solution)/shard_map/all_to_all | solution.py:76
  368.6 33.5 %all-to-all-start.8 = ((bf16[32,256,64]{1,2,0:T(8,128)(2,1)}), bf16[32,256,64]{1,2,0:T(8,128)(2,1)S(1)}, u32[]{:S(2)}, u32[]{:S(2)}) async-start(bf16[32,256,64]{1,2,0:T(8,128)(2,1)} %broadcast_in_dim.8), calls=%async_computation.8 | async-start | bytes 2097152 | tf_op jit(solution)/shard_map/all_to_all | solution.py:32
  373.6 2.1 copy-start.1
  373.6 2.1 copy-start.3
Sparse Core Ops, SparseCore 0:
  11.7 66.3 all-gather.4
  162.6 59.0 all-gather.6
where the time goes:
time: 411 us; the launch traced here: 410 us
  waiting for transfers between devices  208 us (51%)
  blocking collectives  104 us (25%)
  starting transfers between devices  54.7 us (13%)
  local copies, waits for them, and re-layouts  15.6 us (4%)
  between operations  14.3 us (3%)
  other arithmetic  8.55 us (2%)
  matrix products  4.65 us (1%)
    all_gather x2, waiting for transfers between devices, side_by_side(): lax.all_gather(both, axis, axis=dim, tiled=True)  95.2 us
    all_gather x2, blocking collectives, per_device(): lax.all_gather(down_bf, ('gr', 'tp'), axis=1, tiled=True)  62.2 us
    all_to_all x3, waiting for transfers between devices, from_everyone(): lax.all_to_all(jnp.broadcast_to(value[None], (count, *value.shape)), axis...  52.9 us
    all_to_all x1, blocking collectives, sum_at_owner(): tiles = lax.all_to_all(in_blocks(value, dim, count), axis, 0, 0, tiled=True)  42 us
    all_to_all x2, waiting for transfers between devices, per_device(): lax.all_to_all(gate_all, 'fs', split_axis=1, concat_axis=0, tiled=True)  33.3 us
    all_to_all x1, waiting for transfers between devices, sum_at_owner(): tiles = lax.all_to_all(in_blocks(value, dim, count), axis, 0, 0, tiled=True)  26.9 us
    all_to_all x3, starting transfers between devices, from_everyone(): lax.all_to_all(jnp.broadcast_to(value[None], (count, *value.shape)), axis...  15.8 us
    all_to_all x2, starting transfers between devices, per_device(): lax.all_to_all(gate_all, 'fs', split_axis=1, concat_axis=0, tiled=True)  15.7 us
  transfers between devices with their start and end apart: 10, of which 7 were waited for; matrix products, arithmetic and copies ran while one was open for 4% of the time, Pallas kernels for 0%

commit v1 on v0

--- a/solution.py
+++ b/solution.py
@@ -69,7 +69,12 @@
         down_bf = down_weight[half_step].astype(jnp.bfloat16)
         gate_all, up_all, down_new = (
             *side_by_side((gate_bf, up_bf), ("gr", "tp"), 1, 0),
-            lax.all_gather(down_bf, ("gr", "tp"), axis=1, tiled=True),
+            jnp.concatenate(
+                lax.all_to_all(
+                    jnp.stack([down_bf] * lax.axis_size(("gr", "tp"))), ("gr", "tp"), 0, 0
+                ),
+                axis=1,
+            ),
         )
         gate_new, up_new = (
             lax.all_to_all(gate_all, "fs", split_axis=1, concat_axis=0, tiled=True),

time: 411 us -> 369 us (0.90)
  the two profiles are of different devices: /device:TPU:8 before, /device:TPU:6 now
where the time goes in v1:
time: 369 us; the launch traced here: 367 us
  waiting for transfers between devices  222 us (60%)
  starting transfers between devices  62.2 us (17%)
  blocking collectives  33.7 us (9%)
  local copies, waits for them, and re-layouts  21.4 us (6%)
  between operations  14.2 us (4%)
  other arithmetic  9.45 us (3%)
  matrix products  4.64 us (1%)
    all_to_all x3, waiting for transfers between devices, from_everyone(): lax.all_to_all(jnp.broadcast_to(value[None], (count, *value.shape)), axis...  57.3 us
    all_gather x2, waiting for transfers between devices, side_by_side(): lax.all_gather(both, axis, axis=dim, tiled=True)  56.4 us
    all_to_all x1, blocking collectives, sum_at_owner(): tiles = lax.all_to_all(in_blocks(value, dim, count), axis, 0, 0, tiled=True)  33.7 us
    all_to_all x2, waiting for transfers between devices, per_device(): lax.all_to_all(gate_all, 'fs', split_axis=1, concat_axis=0, tiled=True)  33.5 us
    all_to_all x2, waiting for transfers between devices, per_device(): lax.all_to_all(up_all, 'fs', split_axis=1, concat_axis=0, tiled=True)  29 us
    all_to_all x1, waiting for transfers between devices, sum_at_owner(): tiles = lax.all_to_all(in_blocks(value, dim, count), axis, 0, 0, tiled=True)  28.4 us
    all_to_all x2, starting transfers between devices, per_device(): lax.all_to_all(jnp.stack([down_bf] * lax.axis_size(('gr', 'tp'))), ('gr',...  19.7 us
    all_to_all x2, waiting for transfers between devices, per_device(): lax.all_to_all(jnp.stack([down_bf] * lax.axis_size(('gr', 'tp'))), ('gr',...  17.2 us
  transfers between devices with their start and end apart: 12, of which 11 were waited for; matrix products, arithmetic and copies ran while one was open for 6% of the time, Pallas kernels for 0%

profile of v1, /device:TPU:6, one launch (start us, length us, event | category | flops | bytes accessed | tf_op | source)
XLA Modules:
  0.0 367.5 jit_solution(1404761374186417758)
XLA Ops:
  8.0 1.0 fusion.26
  9.7 0.9 convert.4
  10.6 0.9 stack.29
  11.5 13.2 %all-to-all-start.4 = ((bf16[16,128,128]{2,1,0:T(8,128)(2,1)}), bf16[16,128,128]{2,1,0:T(8,128)(2,1)S(1)}, u32[]{:S(2)}, u32[]{:S(2)}) async-start(bf16[16,128,128]{2,1,0:T(8,128)(2,1)} %stack.29), calls=%async_computation.4 | async-start | bytes 1048576 | tf_op jit(solution)/shard_map/all_to_all | solution.py:73
  24.7 54.0 %all-gather.3.cloned.1.call-done = bf16[128,4096]{1,0:T(8,128)(2,1)} async-done(((bf16[128,256]{1,0:T(8,128)(2,1)}), bf16[128,4096]{1,0:T(8,128)(2,1)}) %all-gather.3.cloned.1.call-update) | async-done | bytes 1048592 | tf_op jit(solution)/shard_map/all_gather | solution.py:11
  78.7 1.3 slice_bitcast_fusion.1
  80.0 0.9 copy.50
  81.0 7.6 %all-to-all-start = ((bf16[64,32,128]{2,0,1:T(8,128)(2,1)}), bf16[64,32,128]{2,0,1:T(8,128)(2,1)S(1)}, u32[]{:S(2)}, u32[]{:S(2)}) async-start(bf16[64,32,128]{2,0,1:T(8,128)(2,1)} %bitcast.111), calls=%async_computation | async-start | bytes 1048576 | tf_op jit(solution)/shard_map/all_to_all | solution.py:80
  88.5 0.9 copy.48
  89.5 16.5 %all-to-all-done = bf16[64,32,128]{2,0,1:T(8,128)(2,1)S(1)} async-done(((bf16[64,32,128]{2,0,1:T(8,128)(2,1)}), bf16[64,32,128]{2,0,1:T(8,128)(2,1)S(1)}, u32[]{:S(2)}, u32[]{:S(2)}) %all-to-all-start) | async-done | bytes 524320 | tf_op jit(solution)/shard_map/all_to_all | solution.py:80
  106.0 5.2 %all-to-all-start.2 = ((bf16[64,32,128]{2,0,1:T(8,128)(2,1)}), bf16[64,32,128]{2,0,1:T(8,128)(2,1)S(1)}, u32[]{:S(2)}, u32[]{:S(2)}) async-start(bf16[64,32,128]{2,0,1:T(8,128)(2,1)} %bitcast.109), calls=%async_computation.2 | async-start | bytes 1048576 | tf_op jit(solution)/shard_map/all_to_all | solution.py:81
  111.2 1.5 copy.34
  113.8 14.7 %all-to-all-done.2 = bf16[64,32,128]{2,0,1:T(8,128)(2,1)S(1)} async-done(((bf16[64,32,128]{2,0,1:T(8,128)(2,1)}), bf16[64,32,128]{2,0,1:T(8,128)(2,1)S(1)}, u32[]{:S(2)}, u32[]{:S(2)}) %all-to-all-start.2) | async-done | bytes 524320 | tf_op jit(solution)/shard_map/all_to_all | solution.py:81
  128.5 0.8 convolution_convert_fusion.1
  129.3 1.3 copy.35
  130.6 4.9 %all-to-all-start.6 = ((bf16[32,256,64]{1,2,0:T(8,128)(2,1)}), bf16[32,256,64]{1,2,0:T(8,128)(2,1)S(1)}, u32[]{:S(2)}, u32[]{:S(2)}) async-start(bf16[32,256,64]{1,2,0:T(8,128)(2,1)} %bitcast.120), calls=%async_computation.6 | async-start | bytes 2097152 | tf_op jit(solution)/shard_map/all_to_all | solution.py:26
  136.3 28.4 %all-to-all-done.6 = bf16[32,256,64]{1,2,0:T(8,128)(2,1)S(1)} async-done(((bf16[32,256,64]{1,2,0:T(8,128)(2,1)}), bf16[32,256,64]{1,2,0:T(8,128)(2,1)S(1)}, u32[]{:S(2)}, u32[]{:S(2)}) %all-to-all-start.6) | async-done | bytes 1048608 | tf_op jit(solution)/shard_map/all_to_all | solution.py:26
  164.7 0.9 stack.31
  165.6 6.4 %all-to-all-start.5 = ((bf16[16,128,128]{2,1,0:T(8,128)(2,1)}), bf16[16,128,128]{2,1,0:T(8,128)(2,1)}, u32[]{:S(2)}, u32[]{:S(2)}) async-start(bf16[16,128,128]{2,1,0:T(8,128)(2,1)} %stack.31), calls=%async_computation.5 | async-start | bytes 1048576 | tf_op jit(solution)/shard_map/all_to_all | solution.py:73
  172.0 1.5 convert_element_type.57
  173.6 0.9 multiply_reduce_fusion.1
  174.5 17.2 %all-to-all-done.5 = bf16[16,128,128]{2,1,0:T(8,128)(2,1)} async-done(((bf16[16,128,128]{2,1,0:T(8,128)(2,1)}), bf16[16,128,128]{2,1,0:T(8,128)(2,1)}, u32[]{:S(2)}, u32[]{:S(2)}) %all-to-all-start.5) | async-done | bytes 524320 | tf_op jit(solution)/shard_map/all_to_all | solution.py:73
  192.3 7.2 %all-to-all-start.7 = ((f32[32,256,1]{1,2,0:T(1,128)}), f32[32,256,1]{1,2,0:T(1,128)S(1)}, u32[]{:S(2)}, u32[]{:S(2)}) async-start(f32[32,256,1]{1,2,0:T(1,128)} %broadcast_in_dim.6), calls=%async_computation.7 | async-start | bytes 65536 | tf_op jit(solution)/shard_map/all_to_all | solution.py:32
  199.6 2.4 all-gather.5.cloned.1.call-done
  201.9 1.3 slice_bitcast_fusion
  203.2 0.9 copy.49
  204.1 5.6 %all-to-all-done.7 = f32[32,256,1]{1,2,0:T(1,128)S(1)} async-done(((f32[32,256,1]{1,2,0:T(1,128)}), f32[32,256,1]{1,2,0:T(1,128)S(1)}, u32[]{:S(2)}, u32[]{:S(2)}) %all-to-all-start.7) | async-done | bytes 32800 | tf_op jit(solution)/shard_map/all_to_all | solution.py:32
  209.7 3.9 %all-to-all-start.1 = ((bf16[64,32,128]{2,0,1:T(8,128)(2,1)}), bf16[64,32,128]{2,0,1:T(8,128)(2,1)S(1)}, u32[]{:S(2)}, u32[]{:S(2)}) async-start(bf16[64,32,128]{2,0,1:T(8,128)(2,1)} %bitcast.110), calls=%async_computation.1 | async-start | bytes 1048576 | tf_op jit(solution)/shard_map/all_to_all | solution.py:80
  213.7 17.0 %all-to-all-done.1 = bf16[64,32,128]{2,0,1:T(8,128)(2,1)S(1)} async-done(((bf16[64,32,128]{2,0,1:T(8,128)(2,1)}), bf16[64,32,128]{2,0,1:T(8,128)(2,1)S(1)}, u32[]{:S(2)}, u32[]{:S(2)}) %all-to-all-start.1) | async-done | bytes 524320 | tf_op jit(solution)/shard_map/all_to_all | solution.py:80
  230.8 1.1 broadcast_in_dim.7
  231.9 4.9 %all-to-all-start.8 = ((bf16[32,256,64]{1,2,0:T(8,128)(2,1)}), bf16[32,256,64]{1,2,0:T(8,128)(2,1)S(1)}, u32[]{:S(2)}, u32[]{:S(2)}) async-start(bf16[32,256,64]{1,2,0:T(8,128)(2,1)} %broadcast_in_dim.7), calls=%async_computation.8 | async-start | bytes 2097152 | tf_op jit(solution)/shard_map/all_to_all | solution.py:32
  236.8 0.9 copy.47
  237.7 28.2 %all-to-all-done.8 = bf16[32,256,64]{1,2,0:T(8,128)(2,1)S(1)} async-done(((bf16[32,256,64]{1,2,0:T(8,128)(2,1)}), bf16[32,256,64]{1,2,0:T(8,128)(2,1)S(1)}, u32[]{:S(2)}, u32[]{:S(2)}) %all-to-all-start.8) | async-done | bytes 1048608 | tf_op jit(solution)/shard_map/all_to_all | solution.py:32
  265.9 4.4 %all-to-all-start.3 = ((bf16[64,32,128]{2,0,1:T(8,128)(2,1)}), bf16[64,32,128]{2,0,1:T(8,128)(2,1)S(1)}, u32[]{:S(2)}, u32[]{:S(2)}) async-start(bf16[64,32,128]{2,0,1:T(8,128)(2,1)} %bitcast.108), calls=%async_computation.3 | async-start | bytes 1048576 | tf_op jit(solution)/shard_map/all_to_all | solution.py:81
  270.3 1.3 copy.33
  271.6 1.5 convolution_bitcast_fusion.1
  273.1 14.3 %all-to-all-done.3 = bf16[64,32,128]{2,0,1:T(8,128)(2,1)S(1)} async-done(((bf16[64,32,128]{2,0,1:T(8,128)(2,1)}), bf16[64,32,128]{2,0,1:T(8,128)(2,1)S(1)}, u32[]{:S(2)}, u32[]{:S(2)}) %all-to-all-start.3) | async-done | bytes 524320 | tf_op jit(solution)/shard_map/all_to_all | solution.py:81
  287.4 1.8 convolution_convert_fusion
  289.2 1.5 copy.36
  290.7 33.7 %all_to_all.105 = bf16[32,256,64]{1,2,0:T(8,128)(2,1)S(1)} all-to-all(bf16[32,256,64]{1,2,0:T(8,128)(2,1)S(1)} %bitcast.121), channel_id=1, replica_groups=mesh['gr'=2,'fs'=32,'tp'=8] {'fs'}, dimensions={0} | all-to-all | bytes 2097152 | tf_op jit(solution)/shard_map/all_to_all | solution.py:26
  324.6 1.1 broadcast_in_dim.8
  325.7 4.4 %all-to-all-start.10 = ((bf16[32,256,64]{1,2,0:T(8,128)(2,1)}), bf16[32,256,64]{1,2,0:T(8,128)(2,1)S(1)}, u32[]{:S(2)}, u32[]{:S(2)}) async-start(bf16[32,256,64]{1,2,0:T(8,128)(2,1)} %broadcast_in_dim.8), calls=%async_computation.10 | async-start | bytes 2097152 | tf_op jit(solution)/shard_map/all_to_all | solution.py:32
  330.1 1.1 pad_maximum_fusion.2
  331.2 2.4 copy.37
  333.6 1.1 pad_maximum_fusion.1
  334.6 1.1 pad_maximum_fusion
  335.7 23.6 %all-to-all-done.10 = bf16[32,256,64]{1,2,0:T(8,128)(2,1)S(1)} async-done(((bf16[32,256,64]{1,2,0:T(8,128)(2,1)}), bf16[32,256,64]{1,2,0:T(8,128)(2,1)S(1)}, u32[]{:S(2)}, u32[]{:S(2)}) %all-to-all-start.10) | async-done | bytes 1048608 | tf_op jit(solution)/shard_map/all_to_all | solution.py:32
  359.2 1.4 copy.38
  (28 shorter events, 4.3 us)
Async XLA Ops:
  7.2 71.6 %all-gather.3.cloned.1.call-start = ((), (), s32[]{:S(2)}) async-start(), calls=%async_computation.11 | async-start | bytes 1114112 | tf_op jit(solution)/shard_map/all_gather | solution.py:11
  11.5 69.5 %all-to-all-start.4 = ((bf16[16,128,128]{2,1,0:T(8,128)(2,1)}), bf16[16,128,128]{2,1,0:T(8,128)(2,1)S(1)}, u32[]{:S(2)}, u32[]{:S(2)}) async-start(bf16[16,128,128]{2,1,0:T(8,128)(2,1)} %stack.29), calls=%async_computation.4 | async-start | bytes 1048576 | tf_op jit(solution)/shard_map/all_to_all | solution.py:73
  81.0 25.0 %all-to-all-start = ((bf16[64,32,128]{2,0,1:T(8,128)(2,1)}), bf16[64,32,128]{2,0,1:T(8,128)(2,1)S(1)}, u32[]{:S(2)}, u32[]{:S(2)}) async-start(bf16[64,32,128]{2,0,1:T(8,128)(2,1)} %bitcast.111), calls=%async_computation | async-start | bytes 1048576 | tf_op jit(solution)/shard_map/all_to_all | solution.py:80
  106.0 7.3 %copy-start = (bf16[64,32,128]{2,0,1:T(8,128)(2,1)}, bf16[64,32,128]{2,0,1:T(8,128)(2,1)S(1)}, u32[]{:S(2)}) copy-start(bf16[64,32,128]{2,0,1:T(8,128)(2,1)S(1)} %all-to-all-done) | copy-start | bytes 1572868
  106.0 22.5 %all-to-all-start.2 = ((bf16[64,32,128]{2,0,1:T(8,128)(2,1)}), bf16[64,32,128]{2,0,1:T(8,128)(2,1)S(1)}, u32[]{:S(2)}, u32[]{:S(2)}) async-start(bf16[64,32,128]{2,0,1:T(8,128)(2,1)} %bitcast.109), calls=%async_computation.2 | async-start | bytes 1048576 | tf_op jit(solution)/shard_map/all_to_all | solution.py:81
  130.6 34.0 %all-to-all-start.6 = ((bf16[32,256,64]{1,2,0:T(8,128)(2,1)}), bf16[32,256,64]{1,2,0:T(8,128)(2,1)S(1)}, u32[]{:S(2)}, u32[]{:S(2)}) async-start(bf16[32,256,64]{1,2,0:T(8,128)(2,1)} %bitcast.120), calls=%async_computation.6 | async-start | bytes 2097152 | tf_op jit(solution)/shard_map/all_to_all | solution.py:26
  135.6 66.4 %all-gather.5.cloned.1.call-start = ((), (), s32[]{:S(2)}) async-start(), calls=%async_computation.12 | async-start | bytes 1114112 | tf_op jit(solution)/shard_map/all_gather | solution.py:11
  165.6 26.1 %all-to-all-start.5 = ((bf16[16,128,128]{2,1,0:T(8,128)(2,1)}), bf16[16,128,128]{2,1,0:T(8,128)(2,1)}, u32[]{:S(2)}, u32[]{:S(2)}) async-start(bf16[16,128,128]{2,1,0:T(8,128)(2,1)} %stack.31), calls=%async_computation.5 | async-start | bytes 1048576 | tf_op jit(solution)/shard_map/all_to_all | solution.py:73
  192.3 17.4 %all-to-all-start.7 = ((f32[32,256,1]{1,2,0:T(1,128)}), f32[32,256,1]{1,2,0:T(1,128)S(1)}, u32[]{:S(2)}, u32[]{:S(2)}) async-start(f32[32,256,1]{1,2,0:T(1,128)} %broadcast_in_dim.6), calls=%async_computation.7 | async-start | bytes 65536 | tf_op jit(solution)/shard_map/all_to_all | solution.py:32
  209.7 21.0 %all-to-all-start.1 = ((bf16[64,32,128]{2,0,1:T(8,128)(2,1)}), bf16[64,32,128]{2,0,1:T(8,128)(2,1)S(1)}, u32[]{:S(2)}, u32[]{:S(2)}) async-start(bf16[64,32,128]{2,0,1:T(8,128)(2,1)} %bitcast.110), calls=%async_computation.1 | async-start | bytes 1048576 | tf_op jit(solution)/shard_map/all_to_all | solution.py:80
  230.8 6.9 %copy-start.2 = (bf16[64,32,128]{2,0,1:T(8,128)(2,1)}, bf16[64,32,128]{2,0,1:T(8,128)(2,1)S(1)}, u32[]{:S(2)}) copy-start(bf16[64,32,128]{2,0,1:T(8,128)(2,1)S(1)} %all-to-all-done.1) | copy-start | bytes 1572868
  231.9 34.0 %all-to-all-start.8 = ((bf16[32,256,64]{1,2,0:T(8,128)(2,1)}), bf16[32,256,64]{1,2,0:T(8,128)(2,1)S(1)}, u32[]{:S(2)}, u32[]{:S(2)}) async-start(bf16[32,256,64]{1,2,0:T(8,128)(2,1)} %broadcast_in_dim.7), calls=%async_computation.8 | async-start | bytes 2097152 | tf_op jit(solution)/shard_map/all_to_all | solution.py:32
  265.9 21.5 %all-to-all-start.3 = ((bf16[64,32,128]{2,0,1:T(8,128)(2,1)}), bf16[64,32,128]{2,0,1:T(8,128)(2,1)S(1)}, u32[]{:S(2)}, u32[]{:S(2)}) async-start(bf16[64,32,128]{2,0,1:T(8,128)(2,1)} %bitcast.108), calls=%async_computation.3 | async-start | bytes 1048576 | tf_op jit(solution)/shard_map/all_to_all | solution.py:81
  325.7 33.5 %all-to-all-start.10 = ((bf16[32,256,64]{1,2,0:T(8,128)(2,1)}), bf16[32,256,64]{1,2,0:T(8,128)(2,1)S(1)}, u32[]{:S(2)}, u32[]{:S(2)}) async-start(bf16[32,256,64]{1,2,0:T(8,128)(2,1)} %broadcast_in_dim.8), calls=%async_computation.10 | async-start | bytes 2097152 | tf_op jit(solution)/shard_map/all_to_all | solution.py:32
  331.2 3.4 copy-start.1
  331.2 3.4 copy-start.3
Sparse Core Ops, SparseCore 0:
  11.7 67.0 all-gather.2
  140.1 61.7 all-gather.4
